TPU v7x, 256 devices: a 4x2x16 block of a 4x16x16 slice. The times are simulated.
256 devices in a mesh: grp: 2 (over y), sp: 16 (over z), tp: 8 (over x, core).
Axes of the slice: x: 4, y: 2, z: 16, core: 2. Of those that a mesh axis runs over, the one named last changes fastest.
The devices are a block of a 4x16x16 slice.
Arguments:
- tokens: bfloat16 [2, 16384, 2048], P('grp', ('sp', 'tp')), parts along dimension 0, may hold values from -6 to 6
- norm_gain: bfloat16 [2048], replicated, may hold values from 0.099609375 to 1.8984375
- w_query: bfloat16 [2048, 1024], P('sp'), may hold values from -0.125 to 0.125
- w_forget: bfloat16 [2048, 1024], P('sp'), may hold values from -0.125 to 0.125
- w_input: bfloat16 [2048, 1024], P('sp'), may hold values from -0.125 to 0.125
- floor_gap: float32 [1024], replicated, may hold values from 1.8310547e-05 to 0.12
- extra_decay: float32 [2, 16384, 16], P('grp', ('sp', 'tp')), parts along dimension 0, may hold values from -1.4 to 0, as said below
- init_state: float32 [2, 16, 64, 64], P('grp'), parts along dimension 0, may hold values from -0.03125 to 0.03125
- head_norm_gain: bfloat16 [1024], replicated, may hold values from 0.099609375 to 1.8984375
- w_output: bfloat16 [1024, 2048], P(None, 'sp'), may hold values from -0.1875 to 0.1875
Outputs:
- mixed: bfloat16 [2, 16384, 2048], P('grp', ('sp', 'tp')), parts along dimension 0
- final_state: float32 [2, 65536], P('grp', ('sp', 'tp')), parts along dimension 0
There are 2 independent parts, one for each index of `grp`. A program takes and returns all parts, laid end to end along the dimension named above; an argument that names none is the same for every part. Nothing has to cross between parts.
Inputs may be any that keep to these rules, and one draw needn't show every extreme that they name: `extra_decay`: no entry is positive.
All inputs are finite; a program needn't handle non-finite values.
Results may differ from a plain program's by a relative error of at most 0.014.
Values may be sent and summed in bfloat16 or wider, within the bound.
A program may use at most 128 MiB of HBM per device.

v0:
```python
import jax
import jax.numpy as jnp
from jax import lax
from jax.sharding import Mesh
from jax.sharding import PartitionSpec as P

HEADS = 16
HEAD = 64
BLOCK = 64
SP_TP = ("sp", "tp_0", "tp_1")
EPSILON = 1e-05


def nothing_yet(value, identity):
    return jax.tree.map(
        lambda a, e: jnp.broadcast_to(jnp.asarray(e, a.dtype), a.shape), value, identity
    )


def entering_2(value, axes, combine, identity):
    before = start = nothing_yet(value, identity)
    total = value
    for axis in reversed(axes):
        peers, mine = (lax.axis_size(axis), lax.axis_index(axis))
        pieces = jax.tree.map(
            lambda part, kind: lax.all_gather(part.astype(kind), axis),
            total,
            (jnp.bfloat16, jnp.bfloat16),
        )
        inside, total = (start, start)
        for k in range(peers):
            passed = k < mine
            total = combine(
                total, jax.tree.map(lambda part, own: part[k].astype(own.dtype), pieces, value)
            )
            inside = jax.tree.map(lambda new, old: jnp.where(passed, new, old), total, inside)
        before = combine(inside, before)
    return before


def prefix_by_axis(value, axes, combine, identity):
    before = start = nothing_yet(value, identity)
    total = value
    for axis in reversed(axes):
        peers, mine = (lax.axis_size(axis), lax.axis_index(axis))
        pieces = lax.all_gather(total, axis)
        inside, total = (start, start)
        for k in reversed(range(peers)):
            passed = k > mine
            total = combine(total, pieces[k])
            inside = jnp.where(passed, total, inside)
        before = combine(inside, before)
    return before


def reduced_to_own(pieces, axes, order):
    inside = pieces.shape[1:]
    pieces = pieces.reshape(*(lax.axis_size(a) for a in axes), *inside)
    pieces = jnp.moveaxis(pieces, order, range(len(axes))).reshape(-1, *inside)
    for k in order:
        pieces = lax.psum_scatter(pieces, axes[k], scatter_dimension=0, tiled=True)
    return pieces[0]


def in_blocks(value, dim, peers):
    lengths = value.shape
    pieces = value.reshape(*lengths[:dim], peers, lengths[dim] // peers, *lengths[dim + 1 :])
    return jnp.moveaxis(pieces, dim, 0)


def summed_rows(value, axes, order, dim):
    peers = lax.axis_size(axes)
    return reduced_to_own(in_blocks(value, dim, peers), axes, order)


def layer_normed(tokens, norm_gain):
    values = tokens.astype(jnp.float32)
    center = values - jnp.mean(values, axis=-1, keepdims=True)
    spread = jnp.mean(center * center, axis=-1, keepdims=True)
    return (center * lax.rsqrt(spread + EPSILON) * norm_gain.astype(jnp.float32)).astype(
        jnp.bfloat16
    )


def gate_terms(query_sum, forget_sum, input_sum, floor_gap, extra_decay):
    query_raw = query_sum.astype(jnp.bfloat16)
    forget_raw = forget_sum.astype(jnp.bfloat16)
    input_raw = input_sum.astype(jnp.bfloat16)
    forget_pre = forget_raw.astype(jnp.float32)
    split_shape = forget_pre.shape[:-1] + (HEADS, HEAD)
    log_keep = jnp.logaddexp(
        jnp.log1p(-floor_gap), jnp.log(floor_gap) + jax.nn.log_sigmoid(forget_pre)
    )
    log_keep = log_keep.reshape(split_shape) + extra_decay[..., None]
    key_gate = (floor_gap * jax.nn.sigmoid(-forget_pre)).reshape(split_shape)
    query = jax.nn.silu(query_raw.astype(jnp.float32)).reshape(split_shape)
    values = input_raw.astype(jnp.float32).reshape(split_shape)
    return (query, key_gate, values, log_keep)


def block_pass(query, key_gate, values, log_keep):
    highest = lax.Precision.HIGHEST
    cumul = jnp.cumsum(log_keep, axis=2)
    q_decayed = query * jnp.exp(cumul)
    key_decayed = key_gate * jnp.exp(-cumul)
    causal = lax.broadcasted_iota(jnp.int32, (BLOCK, BLOCK), 0) >= lax.broadcasted_iota(
        jnp.int32, (BLOCK, BLOCK), 1
    )
    scores = jnp.einsum("snthd,snuhd->snhtu", q_decayed, key_decayed, precision=highest)
    scores = jnp.where(causal, scores, 0.0)
    within = jnp.einsum("snhtu,snuhe->snthe", scores, values, precision=highest)
    totals = cumul[:, :, -1]
    k_tail = key_gate * jnp.exp(totals[:, :, None] - cumul)
    block_state = jnp.einsum("snthd,snthe->snhde", k_tail, values, precision=highest)
    return (q_decayed, within, totals, block_state)


def linked_advance(earlier, later):
    return (earlier[0] + later[0], jnp.exp(later[0])[..., None] * earlier[1] + later[1])


def add_logs(earlier, later):
    return earlier + later


def read_out(q_global, leading_logarithm, prefix_state, init_part):
    carried = jnp.exp(leading_logarithm)[..., None] * init_part + prefix_state
    added = jnp.einsum("snthd,shde->snthe", q_global, carried, precision=lax.Precision.HIGHEST)
    return (carried, added)


def body(
    tokens,
    norm_gain,
    w_query,
    w_forget,
    w_input,
    floor_gap,
    extra_decay,
    init_state,
    head_norm_gain,
    w_output,
):
    normed = layer_normed(tokens, norm_gain)
    seqs, span = (tokens.shape[0], tokens.shape[1])

    def add_rows(piece):
        return jnp.dot(normed, piece, preferred_element_type=jnp.float32)

    query_sum = add_rows(lax.all_gather(w_query, "sp", axis=0, tiled=True))
    forget_sum = add_rows(lax.all_gather(w_forget, "sp", axis=0, tiled=True))
    input_sum = add_rows(lax.all_gather(w_input, "sp", axis=0, tiled=True))
    query, key_gate, values, log_keep = gate_terms(
        query_sum, forget_sum, input_sum, floor_gap, extra_decay
    )
    blocks = span // BLOCK
    blocked = (seqs, blocks, BLOCK, HEADS, HEAD)
    q_decayed, within, totals, block_state = block_pass(
        query.reshape(blocked),
        key_gate.reshape(blocked),
        values.reshape(blocked),
        log_keep.reshape(blocked),
    )
    running_state = jnp.zeros((seqs, HEADS, HEAD, HEAD), jnp.float32)
    running_log = jnp.zeros((seqs, HEADS, HEAD), jnp.float32)
    entering_list = []
    offset_list = []
    for number in range(blocks):
        entering_list.append(running_state)
        offset_list.append(running_log)
        running_state = (
            jnp.exp(totals[:, number])[..., None] * running_state + block_state[:, number]
        )
        running_log = running_log + totals[:, number]
    entering = jnp.stack(entering_list, axis=1)
    offsets = jnp.stack(offset_list, axis=1)
    local_out = within + jnp.einsum(
        "snthd,snhde->snthe", q_decayed, entering, precision=lax.Precision.HIGHEST
    )
    q_global = q_decayed * jnp.exp(offsets[:, :, None])
    leading_logarithm, prefix_state = entering_2(
        (running_log, running_state),
        SP_TP,
        linked_advance,
        (jnp.zeros_like(running_log), jnp.zeros_like(running_state)),
    )
    carried, added = read_out(q_global, leading_logarithm, prefix_state, init_state)
    flat_total = HEADS * HEAD * HEAD
    piece_count = flat_total // lax.axis_size(SP_TP)
    piece_start = lax.axis_index(SP_TP) * piece_count
    later_log = prefix_by_axis(running_log, SP_TP, add_logs, jnp.zeros_like(running_log))
    surviving = (jnp.exp(later_log)[..., None] * running_state).reshape(seqs, flat_total)
    summed = summed_rows(surviving.astype(jnp.bfloat16), SP_TP, (2, 0, 1), 1).astype(jnp.float32)
    initial_part = (
        jnp.exp(leading_logarithm + running_log + later_log)[..., None] * init_state
    ).reshape(seqs, flat_total)
    final_state = lax.dynamic_slice_in_dim(initial_part, piece_start, piece_count, 1) + summed
    recurrent = (local_out + added).reshape(seqs, span, HEADS, HEAD)
    average_power = jnp.mean(recurrent * recurrent, axis=-1, keepdims=True)
    scaled = (
        recurrent
        * lax.rsqrt(average_power + EPSILON)
        * head_norm_gain.astype(jnp.float32).reshape(HEADS, HEAD)
    )
    gated = scaled.reshape(seqs, span, HEADS * HEAD).astype(jnp.bfloat16)
    mixed = jnp.dot(
        gated,
        lax.all_gather(w_output, "sp", axis=1, tiled=True),
        preferred_element_type=jnp.float32,
    ).astype(jnp.bfloat16)
    return (mixed, final_state)


def solution(mesh):
    torus = Mesh(
        mesh.devices.reshape(mesh.shape["grp"], mesh.shape["sp"], 4, 2),
        ("grp", "sp", "tp_0", "tp_1"),
    )
    in_specs = (
        P("grp", SP_TP, None),
        P(),
        P("sp", None),
        P("sp", None),
        P("sp", None),
        P(),
        P("grp", SP_TP, None),
        P("grp", None, None, None),
        P(),
        P(None, "sp"),
    )
    out_specs = (P("grp", SP_TP, None), P("grp", SP_TP))
    return jax.shard_map(body, mesh=torus, in_specs=in_specs, out_specs=out_specs, check_vma=False)
```

profile of v0, /device:TPU:36, one launch (start us, length us, event | category | flops | bytes accessed | tf_op | source)
XLA Modules:
  0.0 588.2 jit_solution(18242492222280507001)
XLA Ops:
  12.4 1.3 fusion.7
  14.5 85.1 %all-gather.10.cloned.1.call-done = bf16[2048,1024]{1,0:T(8,128)(2,1)} async-done(((bf16[128,1024]{1,0:T(8,128)(2,1)}), bf16[2048,1024]{1,0:T(8,128)(2,1)}) %all-gather.10.cloned.1.call-update) | async-done | bytes 4194320 | tf_op jit(solution)/shard_map/all_gather | solution.py:151
  99.6 3.8 add_select_fusion
  104.2 1.9 all_gather.51
  106.1 1.9 all_gather.58
  108.5 10.8 %all_gather.52 = bf16[4,1,16,64]{3,2,1,0:T(8,128)(2,1)S(1)} all-gather(bf16[1,1,16,64]{3,2,1,0:T(8,128)(2,1)S(1)} %get-tuple-element.47), channel_id=1, replica_groups=mesh['grp'=2,'sp'=16,'tp_0'=4,'tp_1'=2] {'tp_0'}, dimensions={0}, use_global_device_ids=true | all-gather | bytes 10240 | tf_op jit(solution)/shard_map/all_gather | solution.py:26
  119.4 11.9 %all_gather.59 = f32[4,1,16,64]{3,2,1,0:T(8,128)S(1)} all-gather(f32[1,1,16,64]{3,2,1,0:T(8,128)S(1)} %slice_add_fusion.18), channel_id=1, replica_groups=mesh['grp'=2,'sp'=16,'tp_0'=4,'tp_1'=2] {'tp_0'}, dimensions={0}, use_global_device_ids=true | all-gather | bytes 20480 | tf_op jit(solution)/shard_map/all_gather | solution.py:46
  131.3 29.1 %all_gather.53 = bf16[16,1,16,64]{3,2,1,0:T(8,128)(2,1)S(1)} all-gather(bf16[1,1,16,64]{3,2,1,0:T(8,128)(2,1)S(1)} %get-tuple-element.37), channel_id=1, replica_groups=mesh['grp'=2,'sp'=16,'tp_0'=4,'tp_1'=2] {'sp'}, dimensions={0}, use_global_device_ids=true | all-gather | bytes 34816 | tf_op jit(solution)/shard_map/all_gather | solution.py:26
  160.4 26.9 %all_gather.60 = f32[16,1,16,64]{3,2,1,0:T(8,128)S(1)} all-gather(f32[1,1,16,64]{3,2,1,0:T(8,128)S(1)} %slice_add_fusion.15), channel_id=1, replica_groups=mesh['grp'=2,'sp'=16,'tp_0'=4,'tp_1'=2] {'sp'}, dimensions={0}, use_global_device_ids=true | all-gather | bytes 69632 | tf_op jit(solution)/shard_map/all_gather | solution.py:46
  188.4 1.3 reshape_reshape.8
  189.7 3.1 divide_multiply_fusion.1
  192.8 1.2 reshape_reshape.7
  194.0 55.5 %all-gather.6.cloned.1.call-done = bf16[2048,1024]{1,0:T(8,128)(2,1)} async-done(((bf16[128,1024]{1,0:T(8,128)(2,1)}), bf16[2048,1024]{1,0:T(8,128)(2,1)}) %all-gather.6.cloned.1.call-update) | async-done | bytes 4194320 | tf_op jit(solution)/shard_map/all_gather | solution.py:152
  249.5 3.0 convolution_convert_fusion.3
  252.8 3.3 fusion.16
  257.3 1.2 add_convert_fusion
  261.2 1.5 fusion.154
  263.6 2.6 all_gather.54
  266.6 14.0 %all_gather.55 = bf16[4,1,16,64,64]{4,3,2,1,0:T(8,128)(2,1)} all-gather(bf16[1,1,16,64,64]{4,3,2,1,0:T(8,128)(2,1)S(1)} %fusion.36), channel_id=1, replica_groups=mesh['grp'=2,'sp'=16,'tp_0'=4,'tp_1'=2] {'tp_0'}, dimensions={0}, use_global_device_ids=true | all-gather | bytes 655360 | tf_op jit(solution)/shard_map/all_gather | solution.py:26
  280.7 2.5 fusion.52
  284.0 1.3 dynamic-slice
  287.2 2.0 broadcast_multiply_fusion.1
  289.2 1.4 reshape.2016
  291.8 2.4 convolution_select_fusion
  295.3 3.0 fusion.1
  298.3 114.6 %all-reduce.6.cloned.1.call-done = bf16[64,1,512]{2,0,1:T(8,128)(2,1)} async-done(((bf16[64,1,512]{2,0,1:T(8,128)(2,1)}), bf16[64,1,512]{2,0,1:T(8,128)(2,1)}) %all-reduce.6.cloned.1.call-update) | async-done | bytes 65552
  413.6 8.3 %all-reduce.3 = bf16[4,1,512]{2,0,1:T(4,128)(2,1)S(1)} all-reduce(bf16[4,1,512]{2,0,1:T(4,128)(2,1)S(1)} %constant_dynamic-slice_fusion), channel_id=4, replica_groups=mesh['grp'=2,'sp'=16,'tp_0'=4,'tp_1'=2] {'tp_0'}, use_global_device_ids=true, to_apply=%region_6.7.clone | all-reduce | flops 2048 | bytes 8192
  423.1 63.5 %all-gather.12.cloned.1.call-done = bf16[16,1,16,64,64]{4,3,2,1,0:T(8,128)(2,1)} async-done(((bf16[1,1,16,64,64]{4,3,2,1,0:T(8,128)(2,1)}), bf16[16,1,16,64,64]{4,3,2,1,0:T(8,128)(2,1)}) %all-gather.12.cloned.1.call-update) | async-done | bytes 2097168 | tf_op jit(solution)/shard_map/all_gather | solution.py:26
  486.6 10.3 %multiply_reduce_fusion = (f32[2,64,16]{1,2,0:T(8,128)S(1)}, f32[1,2,64,16,64]{2,4,3,1,0:T(8,128)}) fusion(f32[1,2,64,16,64]{2,4,3,1,0:T(8,128)} %fusion.1, f32[2,64,16,64]{3,2,1,0:T(8,128)S(1)} %copy-done.3, f32[1,16,64,64]{3,2,1,0:T(8,128)} %param.17, bf16[16,1,16,64,64]{4,3,2,1,0:T(8,128)(2,1)} %all-gather.12.cloned.1.call-done, ...), kind=kOutput, calls=%fused_computation.33 | convolution fusion | flops 107018240 | bytes 4829206 | tf_op jit(solution)/shard_map/snthd,shde->snthe/dot_general | solution.py:128
  497.0 1.7 copy.73
  499.4 78.2 %all-gather.14.cloned.1.call-done = bf16[1024,2048]{1,0:T(8,128)(2,1)} async-done(((bf16[1024,128]{1,0:T(8,128)(2,1)}), bf16[1024,2048]{1,0:T(8,128)(2,1)}) %all-gather.14.cloned.1.call-update) | async-done | bytes 4194320 | tf_op jit(solution)/shard_map/all_gather | solution.py:208
  577.6 3.7 fusion
  (96 shorter events, 20.7 us)
Async XLA Ops:
  7.2 92.5 %all-gather.10.cloned.1.call-start = ((), (), s32[]{:S(2)}) async-start(), calls=%async_computation.3 | async-start | bytes 4456448 | tf_op jit(solution)/shard_map/all_gather | solution.py:151
  8.0 181.7 %all-gather.8.cloned.1.call-start = ((), (), s32[]{:S(2)}) async-start(), calls=%async_computation.2 | async-start | bytes 4456448 | tf_op jit(solution)/shard_map/all_gather | solution.py:150
  8.8 240.7 %all-gather.6.cloned.1.call-start = ((), (), s32[]{:S(2)}) async-start(), calls=%async_computation.1 | async-start | bytes 4456448 | tf_op jit(solution)/shard_map/all_gather | solution.py:152
  9.6 271.0 %reduce-scatter.4.cloned.1.call-start = ((), (), s32[]{:S(2)}) async-start(), calls=%async_computation.6 | async-start | bytes 196608 | tf_op jit(solution)/shard_map/reduce_scatter | solution.py:61
  10.4 93.0 %copy-start.9 = (f32[2048]{0:T(1024)}, f32[2048]{0:T(1024)S(1)}, u32[]{:S(2)}) copy-start(f32[2048]{0:T(1024)S(1)} %convert_element_type.904) | copy-start | bytes 24580
  12.4 91.0 %copy-start.12 = (f32[128]{0:T(128)}, f32[128]{0:T(128)S(1)}, u32[]{:S(2)}) copy-start(f32[128]{0:T(128)S(1)} %broadcast_multiply_fusion.2) | copy-start | bytes 1540
  13.8 89.7 %copy-start.15 = (f32[128]{0:T(128)}, f32[128]{0:T(128)S(1)}, u32[]{:S(2)}) copy-start(f32[128]{0:T(128)S(1)} %add_rsqrt_fusion.1) | copy-start | bytes 1540
  103.4 86.3 %copy-start.1 = (bf16[1,128,2048]{2,1,0:T(8,128)(2,1)S(1)}, bf16[1,128,2048]{2,1,0:T(8,128)(2,1)}, u32[]{:S(2)}) copy-start(bf16[1,128,2048]{2,1,0:T(8,128)(2,1)} %param.10) | copy-start | bytes 1572868
  189.7 59.8 %copy-start.10 = (f32[2048]{0:T(1024)S(1)}, f32[2048]{0:T(1024)}, u32[]{:S(2)}) copy-start(f32[2048]{0:T(1024)} %copy-done.9) | copy-start | bytes 24580
  189.7 59.8 %copy-start.13 = (f32[128]{0:T(128)S(1)}, f32[128]{0:T(128)}, u32[]{:S(2)}) copy-start(f32[128]{0:T(128)} %copy-done.12) | copy-start | bytes 1540
  189.7 59.8 %copy-start.16 = (f32[128]{0:T(128)S(1)}, f32[128]{0:T(128)}, u32[]{:S(2)}) copy-start(f32[128]{0:T(128)} %copy-done.15) | copy-start | bytes 1540
  260.0 27.1 %copy-start.4 = (f32[16,64]{1,0:T(8,128)S(1)}, f32[16,64]{1,0:T(8,128)}, u32[]{:S(2)}) copy-start(f32[16,64]{1,0:T(8,128)} %get-tuple-element.2) | copy-start | bytes 12292
  260.2 25.1 %copy-start.14 = (u32[256]{0:T(256)S(1)}, u32[256]{0:T(256)}, u32[]{:S(2)}) copy-start(u32[256]{0:T(256)} %constant.88) | copy-start | bytes 3076
  260.2 25.7 %copy-start.11 = (bf16[1024]{0:T(1024)(128)(2,1)S(1)}, bf16[1024]{0:T(1024)(128)(2,1)}, u32[]{:S(2)}) copy-start(bf16[1024]{0:T(1024)(128)(2,1)} %param.18) | copy-start | bytes 6148
  261.2 29.4 %copy-start.6 = (f32[16,64]{1,0:T(8,128)S(1)}, f32[16,64]{1,0:T(8,128)}, u32[]{:S(2)}) copy-start(f32[16,64]{1,0:T(8,128)} %get-tuple-element.4) | copy-start | bytes 12292
  261.2 30.0 %copy-start.5 = (f32[16,64]{1,0:T(8,128)S(1)}, f32[16,64]{1,0:T(8,128)}, u32[]{:S(2)}) copy-start(f32[16,64]{1,0:T(8,128)} %get-tuple-element.5) | copy-start | bytes 12292
  261.2 30.6 %copy-start = (f32[2,64,16,64]{3,2,1,0:T(8,128)S(1)}, f32[2,64,16,64]{3,2,1,0:T(8,128)}, u32[]{:S(2)}) copy-start(f32[2,64,16,64]{3,2,1,0:T(8,128)} %get-tuple-element.13) | copy-start | bytes 1572868
  263.5 149.4 %all-reduce.6.cloned.1.call-start = ((), (), s32[]{:S(2)}) async-start(), calls=%async_computation.7 | async-start | bytes 131072
  280.6 206.0 %all-gather.12.cloned.1.call-start = ((), (), s32[]{:S(2)}) async-start(), calls=%async_computation.4 | async-start | bytes 4456448 | tf_op jit(solution)/shard_map/all_gather | solution.py:26
  283.2 294.4 %all-gather.14.cloned.1.call-start = ((), (), s32[]{:S(2)}) async-start(), calls=%async_computation.5 | async-start | bytes 4456448 | tf_op jit(solution)/shard_map/all_gather | solution.py:208
  290.6 4.7 copy-start.2
  291.8 194.8 %copy-start.8 = (f32[16,64]{1,0:T(8,128)S(1)}, f32[16,64]{1,0:T(8,128)}, u32[]{:S(2)}) copy-start(f32[16,64]{1,0:T(8,128)} %get-tuple-element.45) | copy-start | bytes 12292
  294.2 192.4 %copy-start.3 = (f32[2,64,16,64]{3,2,1,0:T(8,128)S(1)}, f32[2,64,16,64]{3,2,1,0:T(8,128)}, u32[]{:S(2)}) copy-start(f32[2,64,16,64]{3,2,1,0:T(8,128)} %get-tuple-element.16) | copy-start | bytes 1572868
  496.9 80.7 %copy-start.7 = (f32[1024]{0:T(1024)S(1)}, f32[1024]{0:T(1024)}, u32[]{:S(2)}) copy-start(f32[1024]{0:T(1024)} %convert_element_type.1001) | copy-start | bytes 12292
Sparse Core Ops, SparseCore 0:
  9.8 89.7 all-gather.9
  101.4 73.5 all-gather.7
  176.8 72.5 all-gather.5
  263.6 13.2 reduce-scatter.3
  280.7 132.1 all-reduce.5
  414.6 72.0 all-gather.11
  488.4 89.1 all-gather.13
where the time goes:
time: 589 us; the launch traced here: 588 us
  waiting for transfers between devices  400 us (68%)
  blocking collectives  107 us (18%)
  matrix products  31.4 us (5%)
  other arithmetic  18.4 us (3%)
  local copies, waits for them, and re-layouts  15.3 us (3%)
  between operations  15.2 us (3%)
    unnamed x8, waiting for transfers between devices  118 us
    all_gather x1, waiting for transfers between devices, body(): forget_sum = add_rows(lax.all_gather(w_forget, 'sp', axis=0, tiled=True))  85.1 us
    all_gather x1, waiting for transfers between devices, body(): lax.all_gather(w_output, 'sp', axis=1, tiled=True)  78.2 us
    all_gather x1, waiting for transfers between devices, entering_2(): lax.all_gather(part.astype(kind), axis)  63.5 us
    all_gather x5, blocking collectives, entering_2(): lax.all_gather(part.astype(kind), axis)  58.3 us
    all_gather x1, waiting for transfers between devices, body(): input_sum = add_rows(lax.all_gather(w_input, 'sp', axis=0, tiled=True))  55.5 us
    all_gather x3, blocking collectives, prefix_by_axis(): pieces = lax.all_gather(total, axis)  40.7 us
  transfers between devices with their start and end apart: 7, of which 5 were waited for; matrix products, arithmetic and copies ran while one was open for 8% of the time, Pallas kernels for 0%

commit v1 on v0

--- a/solution.py
+++ b/solution.py
@@ -1,3 +1,4 @@
+import functools
 import jax
 import jax.numpy as jnp
 from jax import lax
@@ -9,6 +10,26 @@
 BLOCK = 64
 SP_TP = ("sp", "tp_0", "tp_1")
 EPSILON = 1e-05
+
+
+def obtain_set(array_in, mesh_ax):
+    sheets = []
+    fan = jax.lax.axis_size(mesh_ax)
+    for c in range(fan):
+        sheets.append((c, (c + 1) % fan))
+    windows = []
+    for c in range(fan):
+        windows.append((c, (c - 1) % fan))
+    b_next, spare = ([array_in], [array_in])
+    for _ in range(fan // 2):
+        b_next.append(jax.lax.ppermute(b_next[-1], mesh_ax, sheets))
+    for _ in range((fan - 1) // 2):
+        spare.append(jax.lax.ppermute(spare[-1], mesh_ax, windows))
+    b_now = jnp.concatenate([*b_next[::-1], *spare[1:]], axis=1)
+    return jnp.roll(b_now, (jax.lax.axis_index(mesh_ax) - fan // 2) * array_in.shape[1], 1)
+
+
+end_orders_in = functools.partial(obtain_set, mesh_ax="sp")
 
 
 def nothing_yet(value, identity):
@@ -203,11 +224,9 @@
         * head_norm_gain.astype(jnp.float32).reshape(HEADS, HEAD)
     )
     gated = scaled.reshape(seqs, span, HEADS * HEAD).astype(jnp.bfloat16)
-    mixed = jnp.dot(
-        gated,
-        lax.all_gather(w_output, "sp", axis=1, tiled=True),
-        preferred_element_type=jnp.float32,
-    ).astype(jnp.bfloat16)
+    mixed = jnp.dot(gated, end_orders_in(w_output), preferred_element_type=jnp.float32).astype(
+        jnp.bfloat16
+    )
     return (mixed, final_state)
 
 

time: 589 us -> 614 us (1.042)
  waiting for transfers between devices: 400 us -> 349 us
  local copies, waits for them, and re-layouts: 15.3 us -> 64.4 us
  starting transfers between devices: 0.44 us -> 26.3 us
    ppermute x0 -> x15, waiting for transfers between devices: none -> 86.4 us  [the longest x8 86.4 us: obtain_set(): b_next.append(jax.lax.ppermute(b_next[-1], mesh_ax, sheets))]
    all_gather x1, waiting for transfers between devices: 85.1 us -> 0.01 us  [body(): forget_sum = add_rows(lax.all_gather(w_forget, 'sp', axis=0, tiled=True))]
    all_gather x1 -> x0, waiting for transfers between devices: 78.2 us -> none  [body(): lax.all_gather(w_output, 'sp', axis=1, tiled=True)]
    unnamed x37 -> x76, local copies, waits for them, and re-layouts: 2.66 us -> 45.1 us
    all_gather x1, waiting for transfers between devices: 0.01 us -> 36.7 us  [body(): query_sum = add_rows(lax.all_gather(w_query, 'sp', axis=0, tiled=True))]
    ppermute x0 -> x15, starting transfers between devices: none -> 25.7 us  [the longest x7 22.8 us: obtain_set(): spare.append(jax.lax.ppermute(spare[-1], mesh_ax, windows))]
    unnamed x8 -> x7, waiting for transfers between devices: 118 us -> 93.1 us
    all_gather x1, waiting for transfers between devices: 55.5 us -> 69.6 us  [body(): input_sum = add_rows(lax.all_gather(w_input, 'sp', axis=0, tiled=True))]
  transfers between devices with their start and end apart: 7 -> 21, of which waited for: 5 -> 11; matrix products, arithmetic and copies ran while one was open for 8% -> 16% of each run, Pallas kernels for 0% -> 0%
where the time goes in v1:
time: 614 us; the launch traced here: 613 us
  waiting for transfers between devices  349 us (57%)
  blocking collectives  107 us (17%)
  local copies, waits for them, and re-layouts  64.4 us (10%)
  matrix products  31.7 us (5%)
  starting transfers between devices  26.3 us (4%)
  other arithmetic  18.3 us (3%)
  between operations  15.4 us (3%)
    unnamed x7, waiting for transfers between devices  93.1 us
    ppermute x8, waiting for transfers between devices, obtain_set(): b_next.append(jax.lax.ppermute(b_next[-1], mesh_ax, sheets))  86.4 us
    all_gather x1, waiting for transfers between devices, body(): input_sum = add_rows(lax.all_gather(w_input, 'sp', axis=0, tiled=True))  69.6 us
    all_gather x1, waiting for transfers between devices, entering_2(): lax.all_gather(part.astype(kind), axis)  63.6 us
    all_gather x5, blocking collectives, entering_2(): lax.all_gather(part.astype(kind), axis)  58.5 us
    unnamed x76, local copies, waits for them, and re-layouts  45.1 us
    all_gather x3, blocking collectives, prefix_by_axis(): pieces = lax.all_gather(total, axis)  40.5 us
    all_gather x1, waiting for transfers between devices, body(): query_sum = add_rows(lax.all_gather(w_query, 'sp', axis=0, tiled=True))  36.7 us
  transfers between devices with their start and end apart: 21, of which 11 were waited for; matrix products, arithmetic and copies ran while one was open for 16% of the time, Pallas kernels for 0%

profile of v1, /device:TPU:36, one launch (start us, length us, event | category | flops | bytes accessed | tf_op | source)
XLA Modules:
  0.0 612.8 jit_solution(17428901384207720806)
XLA Ops:
  9.7 2.9 collective-permute-start
  12.6 26.2 %collective-permute-done = bf16[1024,128]{1,0:T(8,128)(2,1)S(1)} collective-permute-done((bf16[1024,128]{1,0:T(8,128)(2,1)}, bf16[1024,128]{1,0:T(8,128)(2,1)S(1)}, u32[]{:S(2)}, u32[]{:S(2)}) %collective-permute-start) | collective-permute-done | bytes 262176 | tf_op jit(solution)/shard_map/ppermute | solution.py:25
  38.8 3.2 collective-permute-start.8
  42.0 11.9 %collective-permute-done.1 = bf16[1024,128]{1,0:T(8,128)(2,1)S(1)} collective-permute-done((bf16[1024,128]{1,0:T(8,128)(2,1)S(1)}, bf16[1024,128]{1,0:T(8,128)(2,1)S(1)}, u32[]{:S(2)}, u32[]{:S(2)}) %collective-permute-start.1) | collective-permute-done | bytes 262176 | tf_op jit(solution)/shard_map/ppermute | solution.py:25
  53.9 3.2 collective-permute-start.9
  57.2 11.7 %collective-permute-done.2 = bf16[1024,128]{1,0:T(8,128)(2,1)S(1)} collective-permute-done((bf16[1024,128]{1,0:T(8,128)(2,1)S(1)}, bf16[1024,128]{1,0:T(8,128)(2,1)S(1)}, u32[]{:S(2)}, u32[]{:S(2)}) %collective-permute-start.2) | collective-permute-done | bytes 262176 | tf_op jit(solution)/shard_map/ppermute | solution.py:25
  68.9 3.2 collective-permute-start.10
  72.1 11.3 %collective-permute-done.3 = bf16[1024,128]{1,0:T(8,128)(2,1)S(1)} collective-permute-done((bf16[1024,128]{1,0:T(8,128)(2,1)S(1)}, bf16[1024,128]{1,0:T(8,128)(2,1)S(1)}, u32[]{:S(2)}, u32[]{:S(2)}) %collective-permute-start.3) | collective-permute-done | bytes 262176 | tf_op jit(solution)/shard_map/ppermute | solution.py:25
  83.5 3.2 collective-permute-start.11
  86.7 11.4 %collective-permute-done.4 = bf16[1024,128]{1,0:T(8,128)(2,1)S(1)} collective-permute-done((bf16[1024,128]{1,0:T(8,128)(2,1)S(1)}, bf16[1024,128]{1,0:T(8,128)(2,1)S(1)}, u32[]{:S(2)}, u32[]{:S(2)}) %collective-permute-start.4) | collective-permute-done | bytes 262176 | tf_op jit(solution)/shard_map/ppermute | solution.py:25
  99.5 3.2 collective-permute-start.12
  102.7 9.7 %collective-permute-done.5 = bf16[1024,128]{1,0:T(8,128)(2,1)S(1)} collective-permute-done((bf16[1024,128]{1,0:T(8,128)(2,1)S(1)}, bf16[1024,128]{1,0:T(8,128)(2,1)S(1)}, u32[]{:S(2)}, u32[]{:S(2)}) %collective-permute-start.5) | collective-permute-done | bytes 262176 | tf_op jit(solution)/shard_map/ppermute | solution.py:25
  113.9 3.3 collective-permute-start.13
  117.1 4.1 collective-permute-done.6
  128.1 3.4 collective-permute-start.14
  144.2 4.6 add_select_fusion
  152.5 36.7 %all-gather.7.cloned.1.call-done = bf16[2048,1024]{1,0:T(8,128)(2,1)} async-done(((bf16[128,1024]{1,0:T(8,128)(2,1)}), bf16[2048,1024]{1,0:T(8,128)(2,1)}) %all-gather.7.cloned.1.call-update) | async-done | bytes 4194320 | tf_op jit(solution)/shard_map/all_gather | solution.py:171
  189.2 3.0 divide_multiply_fusion.1
  194.0 69.6 %all-gather.5.cloned.1.call-done = bf16[2048,1024]{1,0:T(8,128)(2,1)} async-done(((bf16[128,1024]{1,0:T(8,128)(2,1)}), bf16[2048,1024]{1,0:T(8,128)(2,1)}) %all-gather.5.cloned.1.call-update) | async-done | bytes 4194320 | tf_op jit(solution)/shard_map/all_gather | solution.py:173
  263.6 2.9 convolution_convert_fusion.2
  269.3 10.8 %all_gather.49 = bf16[4,1,16,64]{3,2,1,0:T(8,128)(2,1)S(1)} all-gather(bf16[1,1,16,64]{3,2,1,0:T(8,128)(2,1)S(1)} %get-tuple-element.47), channel_id=1, replica_groups=mesh['grp'=2,'sp'=16,'tp_0'=4,'tp_1'=2] {'tp_0'}, dimensions={0}, use_global_device_ids=true | all-gather | bytes 10240 | tf_op jit(solution)/shard_map/all_gather | solution.py:47
  280.2 3.3 fusion.23
  288.1 29.0 %all_gather.50 = bf16[16,1,16,64]{3,2,1,0:T(8,128)(2,1)S(1)} all-gather(bf16[1,1,16,64]{3,2,1,0:T(8,128)(2,1)S(1)} %get-tuple-element.37), channel_id=1, replica_groups=mesh['grp'=2,'sp'=16,'tp_0'=4,'tp_1'=2] {'sp'}, dimensions={0}, use_global_device_ids=true | all-gather | bytes 34816 | tf_op jit(solution)/shard_map/all_gather | solution.py:47
  318.9 12.0 %all_gather.55 = f32[4,1,16,64]{3,2,1,0:T(8,128)S(1)} all-gather(f32[1,1,16,64]{3,2,1,0:T(8,128)S(1)} %slice_add_fusion.18), channel_id=1, replica_groups=mesh['grp'=2,'sp'=16,'tp_0'=4,'tp_1'=2] {'tp_0'}, dimensions={0}, use_global_device_ids=true | all-gather | bytes 20480 | tf_op jit(solution)/shard_map/all_gather | solution.py:67
  330.9 26.7 %all_gather.56 = f32[16,1,16,64]{3,2,1,0:T(8,128)S(1)} all-gather(f32[1,1,16,64]{3,2,1,0:T(8,128)S(1)} %slice_add_fusion.15), channel_id=1, replica_groups=mesh['grp'=2,'sp'=16,'tp_0'=4,'tp_1'=2] {'sp'}, dimensions={0}, use_global_device_ids=true | all-gather | bytes 69632 | tf_op jit(solution)/shard_map/all_gather | solution.py:67
  368.4 14.6 %all_gather.52 = bf16[4,1,16,64,64]{4,3,2,1,0:T(8,128)(2,1)} all-gather(bf16[1,1,16,64,64]{4,3,2,1,0:T(8,128)(2,1)S(1)} %fusion.43), channel_id=1, replica_groups=mesh['grp'=2,'sp'=16,'tp_0'=4,'tp_1'=2] {'tp_0'}, dimensions={0}, use_global_device_ids=true | all-gather | bytes 655360 | tf_op jit(solution)/shard_map/all_gather | solution.py:47
  423.5 3.1 fusion.8
  426.7 90.8 %all-reduce.6.cloned.1.call-done = bf16[64,1,512]{2,0,1:T(8,128)(2,1)} async-done(((bf16[64,1,512]{2,0,1:T(8,128)(2,1)}), bf16[64,1,512]{2,0,1:T(8,128)(2,1)}) %all-reduce.6.cloned.1.call-update) | async-done | bytes 65552
  518.1 8.3 %all-reduce.3 = bf16[4,1,512]{2,0,1:T(4,128)(2,1)S(1)} all-reduce(bf16[4,1,512]{2,0,1:T(4,128)(2,1)S(1)} %constant_dynamic-slice_fusion), channel_id=4, replica_groups=mesh['grp'=2,'sp'=16,'tp_0'=4,'tp_1'=2] {'tp_0'}, use_global_device_ids=true, to_apply=%region_6.7.clone | all-reduce | flops 2048 | bytes 8192
  527.7 63.6 %all-gather.11.cloned.1.call-done = bf16[16,1,16,64,64]{4,3,2,1,0:T(8,128)(2,1)} async-done(((bf16[1,1,16,64,64]{4,3,2,1,0:T(8,128)(2,1)}), bf16[16,1,16,64,64]{4,3,2,1,0:T(8,128)(2,1)}) %all-gather.11.cloned.1.call-update) | async-done | bytes 2097168 | tf_op jit(solution)/shard_map/all_gather | solution.py:47
  591.3 9.7 %multiply_reduce_fusion = (f32[2,64,16]{1,2,0:T(8,128)S(1)}, f32[1,2,64,16,64]{2,4,3,1,0:T(8,128)S(1)}) fusion(f32[1,2,64,16,64]{2,4,3,1,0:T(8,128)S(1)} %fusion.8, f32[2,64,16,64]{3,2,1,0:T(8,128)} %get-tuple-element.16, f32[1,16,64,64]{3,2,1,0:T(8,128)} %param.17, bf16[16,1,16,64,64]{4,3,2,1,0:T(8,128)(2,1)} %all-gather.11.cloned.1.call-done, ...), kind=kOutput, calls=%fused_computation.35 | convolution fusion | flops 107018240 | bytes 4829206 | tf_op jit(solution)/shard_map/snthd,shde->snthe/dot_general | solution.py:149
  602.2 3.7 fusion.5
  (163 shorter events, 92.9 us)
Async XLA Ops:
  7.2 137.0 %copy-start.1 = (bf16[1,128,2048]{2,1,0:T(8,128)(2,1)S(1)}, bf16[1,128,2048]{2,1,0:T(8,128)(2,1)}, u32[]{:S(2)}) copy-start(bf16[1,128,2048]{2,1,0:T(8,128)(2,1)} %param.10) | copy-start | bytes 1572868
  7.2 137.0 %copy-start.20 = (f32[1024]{0:T(1024)S(1)}, f32[1024]{0:T(1024)}, u32[]{:S(2)}) copy-start(f32[1024]{0:T(1024)} %param.15) | copy-start | bytes 12292
  7.2 137.0 %all-gather.9.cloned.1.call-start = ((), (), s32[]{:S(2)}) async-start(), calls=%async_computation.3 | async-start | bytes 4456448 | tf_op jit(solution)/shard_map/all_gather | solution.py:172
  8.0 181.2 %all-gather.7.cloned.1.call-start = ((), (), s32[]{:S(2)}) async-start(), calls=%async_computation.2 | async-start | bytes 4456448 | tf_op jit(solution)/shard_map/all_gather | solution.py:171
  8.8 254.8 %all-gather.5.cloned.1.call-start = ((), (), s32[]{:S(2)}) async-start(), calls=%async_computation.1 | async-start | bytes 4456448 | tf_op jit(solution)/shard_map/all_gather | solution.py:173
  9.6 373.5 %reduce-scatter.4.cloned.1.call-start = ((), (), s32[]{:S(2)}) async-start(), calls=%async_computation.5 | async-start | bytes 196608 | tf_op jit(solution)/shard_map/reduce_scatter | solution.py:82
  9.7 29.1 %collective-permute-start = (bf16[1024,128]{1,0:T(8,128)(2,1)}, bf16[1024,128]{1,0:T(8,128)(2,1)S(1)}, u32[]{:S(2)}, u32[]{:S(2)}) collective-permute-start(bf16[1024,128]{1,0:T(8,128)(2,1)} %param.19), channel_id=1, source_target_pairs={{0,8},{8,16},{16,24},{24,32},{32,40},{40,48},{48,56},{56,64},{64,7... | collective-permute-start | bytes 786440 | tf_op jit(solution)/shard_map/ppermute | solution.py:25
  38.8 110.1 %copy-start.3 = (bf16[1024,128]{1,0:T(8,128)(2,1)}, bf16[1024,128]{1,0:T(8,128)(2,1)S(1)}, u32[]{:S(2)}) copy-start(bf16[1024,128]{1,0:T(8,128)(2,1)S(1)} %collective-permute-done) | copy-start | bytes 786436
  38.8 15.1 %collective-permute-start.1 = (bf16[1024,128]{1,0:T(8,128)(2,1)S(1)}, bf16[1024,128]{1,0:T(8,128)(2,1)S(1)}, u32[]{:S(2)}, u32[]{:S(2)}) collective-permute-start(bf16[1024,128]{1,0:T(8,128)(2,1)S(1)} %collective-permute-done), channel_id=1, source_target_pairs={{0,8},{8,16},{16,24},{24,32},{32,40},{40,48},{48,56},{56,64},{64,7... | collective-permute-start | bytes 786440 | tf_op jit(solution)/shard_map/ppermute | solution.py:25
  38.8 15.2 %collective-permute-start.8 = (bf16[1024,128]{1,0:T(8,128)(2,1)}, bf16[1024,128]{1,0:T(8,128)(2,1)S(1)}, u32[]{:S(2)}, u32[]{:S(2)}) collective-permute-start(bf16[1024,128]{1,0:T(8,128)(2,1)} %param.19), channel_id=1, source_target_pairs={{0,120},{8,0},{16,8},{24,16},{32,24},{40,32},{48,40},{56,48},{64,5... | collective-permute-start | bytes 786440 | tf_op jit(solution)/shard_map/ppermute | solution.py:27
  53.9 94.9 %copy-start.5 = (bf16[1024,128]{1,0:T(8,128)(2,1)}, bf16[1024,128]{1,0:T(8,128)(2,1)S(1)}, u32[]{:S(2)}) copy-start(bf16[1024,128]{1,0:T(8,128)(2,1)S(1)} %collective-permute-done.1) | copy-start | bytes 786436
  53.9 15.0 %collective-permute-start.2 = (bf16[1024,128]{1,0:T(8,128)(2,1)S(1)}, bf16[1024,128]{1,0:T(8,128)(2,1)S(1)}, u32[]{:S(2)}, u32[]{:S(2)}) collective-permute-start(bf16[1024,128]{1,0:T(8,128)(2,1)S(1)} %collective-permute-done.1), channel_id=1, source_target_pairs={{0,8},{8,16},{16,24},{24,32},{32,40},{40,48},{48,56},{56,64},{64,7... | collective-permute-start | bytes 786440 | tf_op jit(solution)/shard_map/ppermute | solution.py:25
  53.9 94.9 %copy-start.4 = (bf16[1024,128]{1,0:T(8,128)(2,1)}, bf16[1024,128]{1,0:T(8,128)(2,1)S(1)}, u32[]{:S(2)}) copy-start(bf16[1024,128]{1,0:T(8,128)(2,1)S(1)} %collective-permute-done.8) | copy-start | bytes 786436
  53.9 15.0 %collective-permute-start.9 = (bf16[1024,128]{1,0:T(8,128)(2,1)S(1)}, bf16[1024,128]{1,0:T(8,128)(2,1)S(1)}, u32[]{:S(2)}, u32[]{:S(2)}) collective-permute-start(bf16[1024,128]{1,0:T(8,128)(2,1)S(1)} %collective-permute-done.8), channel_id=1, source_target_pairs={{0,120},{8,0},{16,8},{24,16},{32,24},{40,32},{48,40},{56,48},{64,5... | collective-permute-start | bytes 786440 | tf_op jit(solution)/shard_map/ppermute | solution.py:27
  68.9 79.9 %copy-start.7 = (bf16[1024,128]{1,0:T(8,128)(2,1)}, bf16[1024,128]{1,0:T(8,128)(2,1)S(1)}, u32[]{:S(2)}) copy-start(bf16[1024,128]{1,0:T(8,128)(2,1)S(1)} %collective-permute-done.2) | copy-start | bytes 786436
  68.9 14.6 %collective-permute-start.3 = (bf16[1024,128]{1,0:T(8,128)(2,1)S(1)}, bf16[1024,128]{1,0:T(8,128)(2,1)S(1)}, u32[]{:S(2)}, u32[]{:S(2)}) collective-permute-start(bf16[1024,128]{1,0:T(8,128)(2,1)S(1)} %collective-permute-done.2), channel_id=1, source_target_pairs={{0,8},{8,16},{16,24},{24,32},{32,40},{40,48},{48,56},{56,64},{64,7... | collective-permute-start | bytes 786440 | tf_op jit(solution)/shard_map/ppermute | solution.py:25
  68.9 79.9 %copy-start.6 = (bf16[1024,128]{1,0:T(8,128)(2,1)}, bf16[1024,128]{1,0:T(8,128)(2,1)S(1)}, u32[]{:S(2)}) copy-start(bf16[1024,128]{1,0:T(8,128)(2,1)S(1)} %collective-permute-done.9) | copy-start | bytes 786436
  68.9 14.6 %collective-permute-start.10 = (bf16[1024,128]{1,0:T(8,128)(2,1)S(1)}, bf16[1024,128]{1,0:T(8,128)(2,1)S(1)}, u32[]{:S(2)}, u32[]{:S(2)}) collective-permute-start(bf16[1024,128]{1,0:T(8,128)(2,1)S(1)} %collective-permute-done.9), channel_id=1, source_target_pairs={{0,120},{8,0},{16,8},{24,16},{32,24},{40,32},{48,40},{56,48},{64,5... | collective-permute-start | bytes 786440 | tf_op jit(solution)/shard_map/ppermute | solution.py:27
  83.5 65.4 %copy-start.10 = (bf16[1024,128]{1,0:T(8,128)(2,1)}, bf16[1024,128]{1,0:T(8,128)(2,1)S(1)}, u32[]{:S(2)}) copy-start(bf16[1024,128]{1,0:T(8,128)(2,1)S(1)} %collective-permute-done.3) | copy-start | bytes 786436
  83.5 14.7 %collective-permute-start.4 = (bf16[1024,128]{1,0:T(8,128)(2,1)S(1)}, bf16[1024,128]{1,0:T(8,128)(2,1)S(1)}, u32[]{:S(2)}, u32[]{:S(2)}) collective-permute-start(bf16[1024,128]{1,0:T(8,128)(2,1)S(1)} %collective-permute-done.3), channel_id=1, source_target_pairs={{0,8},{8,16},{16,24},{24,32},{32,40},{40,48},{48,56},{56,64},{64,7... | collective-permute-start | bytes 786440 | tf_op jit(solution)/shard_map/ppermute | solution.py:25
  83.5 65.4 %copy-start.8 = (bf16[1024,128]{1,0:T(8,128)(2,1)}, bf16[1024,128]{1,0:T(8,128)(2,1)S(1)}, u32[]{:S(2)}) copy-start(bf16[1024,128]{1,0:T(8,128)(2,1)S(1)} %collective-permute-done.10) | copy-start | bytes 786436
  83.5 16.0 %collective-permute-start.11 = (bf16[1024,128]{1,0:T(8,128)(2,1)S(1)}, bf16[1024,128]{1,0:T(8,128)(2,1)S(1)}, u32[]{:S(2)}, u32[]{:S(2)}) collective-permute-start(bf16[1024,128]{1,0:T(8,128)(2,1)S(1)} %collective-permute-done.10), channel_id=1, source_target_pairs={{0,120},{8,0},{16,8},{24,16},{32,24},{40,32},{48,40},{56,48},{64,5... | collective-permute-start | bytes 786440 | tf_op jit(solution)/shard_map/ppermute | solution.py:27
  98.1 14.3 %collective-permute-start.5 = (bf16[1024,128]{1,0:T(8,128)(2,1)S(1)}, bf16[1024,128]{1,0:T(8,128)(2,1)S(1)}, u32[]{:S(2)}, u32[]{:S(2)}) collective-permute-start(bf16[1024,128]{1,0:T(8,128)(2,1)S(1)} %collective-permute-done.4), channel_id=1, source_target_pairs={{0,8},{8,16},{16,24},{24,32},{32,40},{40,48},{48,56},{56,64},{64,7... | collective-permute-start | bytes 786440 | tf_op jit(solution)/shard_map/ppermute | solution.py:25
  99.5 14.4 %collective-permute-start.12 = (bf16[1024,128]{1,0:T(8,128)(2,1)S(1)}, bf16[1024,128]{1,0:T(8,128)(2,1)S(1)}, u32[]{:S(2)}, u32[]{:S(2)}) collective-permute-start(bf16[1024,128]{1,0:T(8,128)(2,1)S(1)} %collective-permute-done.11), channel_id=1, source_target_pairs={{0,120},{8,0},{16,8},{24,16},{32,24},{40,32},{48,40},{56,48},{64,5... | collective-permute-start | bytes 786440 | tf_op jit(solution)/shard_map/ppermute | solution.py:27
  112.4 8.8 %collective-permute-start.6 = (bf16[1024,128]{1,0:T(8,128)(2,1)S(1)}, bf16[1024,128]{1,0:T(8,128)(2,1)}, u32[]{:S(2)}, u32[]{:S(2)}) collective-permute-start(bf16[1024,128]{1,0:T(8,128)(2,1)S(1)} %collective-permute-done.5), channel_id=1, source_target_pairs={{0,8},{8,16},{16,24},{24,32},{32,40},{40,48},{48,56},{56,64},{64,7... | collective-permute-start | bytes 786440 | tf_op jit(solution)/shard_map/ppermute | solution.py:25
  113.9 14.2 %collective-permute-start.13 = (bf16[1024,128]{1,0:T(8,128)(2,1)S(1)}, bf16[1024,128]{1,0:T(8,128)(2,1)}, u32[]{:S(2)}, u32[]{:S(2)}) collective-permute-start(bf16[1024,128]{1,0:T(8,128)(2,1)S(1)} %collective-permute-done.12), channel_id=1, source_target_pairs={{0,120},{8,0},{16,8},{24,16},{32,24},{40,32},{48,40},{56,48},{64,5... | collective-permute-start | bytes 786440 | tf_op jit(solution)/shard_map/ppermute | solution.py:27
  121.2 10.2 %collective-permute-start.7 = (bf16[1024,128]{1,0:T(8,128)(2,1)}, bf16[1024,128]{1,0:T(8,128)(2,1)}, u32[]{:S(2)}, u32[]{:S(2)}) collective-permute-start(bf16[1024,128]{1,0:T(8,128)(2,1)} %collective-permute-done.6), channel_id=1, source_target_pairs={{0,8},{8,16},{16,24},{24,32},{32,40},{40,48},{48,56},{56,64},{64,7... | collective-permute-start | bytes 786440 | tf_op jit(solution)/shard_map/ppermute | solution.py:25
  128.1 261.2 %collective-permute-start.14 = (bf16[1024,128]{1,0:T(8,128)(2,1)}, bf16[1024,128]{1,0:T(8,128)(2,1)}, u32[]{:S(2)}, u32[]{:S(2)}) collective-permute-start(bf16[1024,128]{1,0:T(8,128)(2,1)} %collective-permute-done.13), channel_id=1, source_target_pairs={{0,120},{8,0},{16,8},{24,16},{32,24},{40,32},{48,40},{56,48},{64,5... | collective-permute-start | bytes 786440 | tf_op jit(solution)/shard_map/ppermute | solution.py:27
  365.4 54.7 %copy-start = (f32[2,64,16,64]{3,2,1,0:T(8,128)S(1)}, f32[2,64,16,64]{3,2,1,0:T(8,128)}, u32[]{:S(2)}) copy-start(f32[2,64,16,64]{3,2,1,0:T(8,128)} %get-tuple-element.13) | copy-start | bytes 1572868
  367.8 149.6 %all-reduce.6.cloned.1.call-start = ((), (), s32[]{:S(2)}) async-start(), calls=%async_computation.6 | async-start | bytes 131072
  383.1 208.1 %all-gather.11.cloned.1.call-start = ((), (), s32[]{:S(2)}) async-start(), calls=%async_computation.4 | async-start | bytes 4456448 | tf_op jit(solution)/shard_map/all_gather | solution.py:47
  418.7 172.6 %copy-start.19 = (f32[16,64]{1,0:T(8,128)S(1)}, f32[16,64]{1,0:T(8,128)}, u32[]{:S(2)}) copy-start(f32[16,64]{1,0:T(8,128)} %exp.349) | copy-start | bytes 12292
  (10 other events, 393.7 us)
Sparse Core Ops, SparseCore 0:
  9.8 103.6 all-gather.8
  115.3 73.8 all-gather.6
  191.0 72.4 all-gather.4
  367.9 13.5 reduce-scatter.3
  383.7 133.6 all-reduce.5
  519.1 72.1 all-gather.10
